TPU v7x, 32 devices: a whole 2x2x4 slice. The times are simulated.
32 devices in a mesh: sp: 8 (over z, x), tp: 4 (over y, core).
Axes of the slice: x: 2, y: 2, z: 4, core: 2. Of those that a mesh axis runs over, the one named last changes fastest.
Arguments:
- q_first: bfloat16 [1536, 512], P('sp', 'tp'), may hold values from -6 to 6
- k_first: bfloat16 [1536, 512], P('sp', 'tp'), may hold values from -6 to 6
- q_second: bfloat16 [1536, 512], P('sp', 'tp'), may hold values from -6 to 6
- k_second: bfloat16 [1536, 512], P('sp', 'tp'), may hold values from -6 to 6
- values: bfloat16 [1536, 1024], P('sp', 'tp'), may hold values from -6 to 6
- lambdas: float32 [8], P('tp'), may hold values from 0.3 to 0.8
- head_gain: float32 [128], replicated, may hold values from 0.1 to 1.9
- out_weight: bfloat16 [1024, 2048], P('tp'), may hold values from -0.1875 to 0.1875
- residual_in: bfloat16 [1536, 2048], P('sp'), may hold values from -6 to 6
- mix_gain: float32 [2048], replicated, may hold values from 0.1 to 1.9
- gate_weight: bfloat16 [2048, 5632], P('sp', 'tp'), may hold values from -0.125 to 0.125
- up_weight: bfloat16 [2048, 5632], P('sp', 'tp'), may hold values from -0.125 to 0.125
- gate_taps: float32 [3, 5632], P(None, 'tp'), may hold values from -3.5 to 3.5
- up_taps: float32 [3, 5632], P(None, 'tp'), may hold values from -3.5 to 3.5
- down_weight: bfloat16 [5632, 2048], P('tp'), may hold values from -0.078125 to 0.078125
Outputs:
- mixed: bfloat16 [1536, 2048], P(('sp', 'tp'))
All inputs are finite; a program needn't handle non-finite values.
Results may differ from a plain program's by a relative error of at most 0.017.
Values may be sent and summed in bfloat16 or wider, within the bound.
A program may use at most 128 MiB of HBM per device.

v0:
```python
import jax
import jax.numpy as jnp
from jax import lax
from jax.sharding import PartitionSpec as P

norm_eps = 1e-06
far_below = -1e30


def passed_along(value, axis, steps):
    count = lax.axis_size(axis)
    initial, last = (max(0, -steps), min(count, count - steps))
    return lax.ppermute(value, axis, [(source, source + steps) for source in range(initial, last)])


def block_span(count, limit):
    return max((width for width in range(1, min(count, limit) + 1) if count % width == 0))


def update(peaks, totals, accum, scores, vals, visible):
    masked = jnp.where(visible, scores, far_below)
    new_peaks = jnp.maximum(peaks, jnp.max(masked, axis=-1))
    fade = jnp.exp(peaks - new_peaks)
    weights = jnp.where(visible, jnp.exp(masked - new_peaks[..., None]), 0.0)
    totals = totals * fade + jnp.sum(weights, axis=-1)
    accum = accum * fade.T[..., None] + jnp.einsum(
        "hqk,khv->qhv", weights.astype(jnp.bfloat16), vals, preferred_element_type=jnp.float32
    )
    return (new_peaks, totals, accum)


def rms_scale(field, gain):
    return field * lax.rsqrt(jnp.mean(field * field, axis=-1, keepdims=True) + norm_eps) * gain


def shards(
    q_first,
    k_first,
    q_second,
    k_second,
    values,
    lambdas,
    head_gain,
    out_weight,
    residual_in,
    mix_gain,
    gate_weight,
    up_weight,
    gate_taps,
    up_taps,
    down_weight,
):
    tok_rows = q_first.shape[0]
    head_count = lambdas.shape[0]
    head_dim = q_first.shape[1] // head_count
    value_dim = values.shape[1] // head_count
    part_rows = tok_rows // lax.axis_size("tp")
    tp_rank = lax.axis_index("tp")
    scale = head_dim ** (-0.5)
    query_pos = lax.axis_index("sp") * tok_rows + jnp.arange(tok_rows, dtype=jnp.int32)
    query_a = q_first.reshape(tok_rows, head_count, head_dim)
    query_b = q_second.reshape(tok_rows, head_count, head_dim)
    peaks_start = jnp.full((head_count, tok_rows), far_below, jnp.float32)
    totals_start = jnp.zeros((head_count, tok_rows), jnp.float32)
    accum_start = jnp.zeros((tok_rows, head_count, value_dim), jnp.float32)
    start = jnp.int32(0)
    keys_a = lax.all_gather(k_first, "sp", axis=0, tiled=True)
    keys_b = lax.all_gather(k_second, "sp", axis=0, tiled=True)
    vals = lax.all_gather(values, "sp", axis=0, tiled=True)
    count = keys_a.shape[0]
    span = block_span(count, 2048)

    def step(index, inner):
        peaks_a, totals_a, accum_a, peaks_b, totals_b, accum_b = inner
        offset = index * span
        block_a = lax.dynamic_slice_in_dim(keys_a, offset, span, 0).reshape(
            span, head_count, head_dim
        )
        block_b = lax.dynamic_slice_in_dim(keys_b, offset, span, 0).reshape(
            span, head_count, head_dim
        )
        block_v = lax.dynamic_slice_in_dim(vals, offset, span, 0).reshape(
            span, head_count, value_dim
        )
        key_pos = start + offset + jnp.arange(span, dtype=jnp.int32)
        visible = (key_pos[None, :] <= query_pos[:, None])[None]
        scores_a = (
            jnp.einsum("qhd,khd->hqk", query_a, block_a, preferred_element_type=jnp.float32) * scale
        )
        scores_b = (
            jnp.einsum("qhd,khd->hqk", query_b, block_b, preferred_element_type=jnp.float32) * scale
        )
        peaks_a, totals_a, accum_a = update(peaks_a, totals_a, accum_a, scores_a, block_v, visible)
        peaks_b, totals_b, accum_b = update(peaks_b, totals_b, accum_b, scores_b, block_v, visible)
        return (peaks_a, totals_a, accum_a, peaks_b, totals_b, accum_b)

    carry = lax.fori_loop(
        0,
        count // span,
        step,
        (peaks_start, totals_start, accum_start, peaks_start, totals_start, accum_start),
    )
    first = carry[2] / carry[1].T[..., None]
    second = carry[5] / carry[4].T[..., None]
    diff_heads = first - lambdas[None, :, None] * second
    head_out = (
        rms_scale(diff_heads, head_gain)
        .astype(jnp.bfloat16)
        .reshape(tok_rows, head_count * value_dim)
    )
    attended = lax.psum_scatter(
        jnp.dot(head_out, out_weight, preferred_element_type=jnp.float32).astype(jnp.bfloat16),
        "tp",
        scatter_dimension=0,
        tiled=True,
    ).astype(jnp.float32)
    own_rows = lax.dynamic_slice_in_dim(residual_in, tp_rank * part_rows, part_rows, 0)
    stream_rows = own_rows.astype(jnp.float32) + attended
    normed_part = rms_scale(stream_rows, mix_gain).astype(jnp.bfloat16)
    ffn_in = lax.all_gather(normed_part, "tp", axis=0, tiled=True)
    gate_pre = jnp.dot(
        ffn_in,
        lax.all_gather(gate_weight, "sp", axis=0, tiled=True),
        preferred_element_type=jnp.float32,
    )
    up_pre = jnp.dot(
        ffn_in,
        lax.all_gather(up_weight, "sp", axis=0, tiled=True),
        preferred_element_type=jnp.float32,
    )
    projected = jnp.stack((gate_pre.astype(jnp.bfloat16), up_pre.astype(jnp.bfloat16)))
    tap_count = gate_taps.shape[0]
    edge = passed_along(projected[:, tok_rows - (tap_count - 1) :], "sp", 1)
    padded = jnp.concatenate((edge, projected), axis=1).astype(jnp.float32)
    taps = jnp.stack((gate_taps, up_taps))
    convolved = taps[:, 0][:, None, :] * padded[:, 0:tok_rows]
    for offset in range(1, tap_count):
        convolved = convolved + taps[:, offset][:, None, :] * padded[:, offset : offset + tok_rows]
    hidden = (jax.nn.silu(convolved[0]) * convolved[1]).astype(jnp.bfloat16)
    down_rows = lax.psum_scatter(
        jnp.dot(hidden, down_weight, preferred_element_type=jnp.float32).astype(jnp.bfloat16),
        "tp",
        scatter_dimension=0,
        tiled=True,
    ).astype(jnp.float32)
    return (stream_rows + down_rows).astype(jnp.bfloat16)


def solution(mesh):
    in_specs = (
        P("sp", "tp"),
        P("sp", "tp"),
        P("sp", "tp"),
        P("sp", "tp"),
        P("sp", "tp"),
        P("tp"),
        P(),
        P("tp", None),
        P("sp", None),
        P(),
        P("sp", "tp"),
        P("sp", "tp"),
        P(None, "tp"),
        P(None, "tp"),
        P("tp", None),
    )
    out_specs = P(("sp", "tp"), None)
    return jax.shard_map(shards, mesh=mesh, in_specs=in_specs, out_specs=out_specs, check_vma=False)
```

profile of v0, /device:TPU:0, one launch (start us, length us, event | category | flops | bytes accessed | tf_op | source)
XLA Modules:
  0.0 361.2 jit_solution(8689654053603012556)
XLA Ops:
  7.4 0.9 iota_compare_fusion
  8.3 33.0 %all_gather.18 = bf16[1536,128]{1,0:T(8,128)(2,1)S(1)} all-gather(bf16[192,128]{1,0:T(8,128)(2,1)} %param.16), channel_id=1, replica_groups=mesh['sp'=8,'tp'=4] {'sp'}, dimensions={0}, use_global_device_ids=true | all-gather | bytes 442368 | tf_op jit(solution)/shard_map/all_gather | solution.py:67
  41.3 0.9 copy.29
  42.2 0.9 copy.28
  43.1 1.8 fusion.55
  45.0 0.0 copy-done.7
  45.0 33.0 %all_gather.20 = bf16[1536,128]{1,0:T(8,128)(2,1)} all-gather(bf16[192,128]{1,0:T(8,128)(2,1)S(1)} %copy-done.7), channel_id=1, replica_groups=mesh['sp'=8,'tp'=4] {'sp'}, dimensions={0}, use_global_device_ids=true | all-gather | bytes 442368 | tf_op jit(solution)/shard_map/all_gather | solution.py:68
  78.0 1.9 copy.33
  79.9 0.9 copy.32
  80.8 0.0 copy-start.6
  80.8 3.2 fusion.54
  84.0 34.0 %all_gather.19 = bf16[1536,256]{1,0:T(8,128)(2,1)} all-gather(bf16[192,256]{1,0:T(8,128)(2,1)S(1)} %copy-done.6), channel_id=1, replica_groups=mesh['sp'=8,'tp'=4] {'sp'}, dimensions={0}, use_global_device_ids=true | all-gather | bytes 884736 | tf_op jit(solution)/shard_map/all_gather | solution.py:69
  118.0 2.3 copy.30
  120.3 3.0 fusion.6
  123.4 0.7 fusion.41
  124.1 0.0 copy-start.11
  124.2 0.8 multiply_reduce_fusion.1
  125.0 0.0 copy-start.9
  125.0 0.0 copy-start.5
  125.0 0.0 copy-done
  125.0 0.0 copy-done.11
  125.0 0.0 copy-start.10
  125.1 1.3 convolution_convert_fusion.3
  126.4 0.0 reduce-scatter.3.cloned.1.call-update
  126.4 0.0 all-gather.3.cloned.1.call-start
  126.4 0.5 all-gather.3.cloned.1.call-update
  127.0 0.0 all-gather.5.cloned.1.call-start
  127.0 0.5 all-gather.5.cloned.1.call-update
  127.6 0.0 reduce-scatter.5.cloned.1.call-start
  127.7 23.4 %reduce-scatter.3.cloned.1.call-done = bf16[48,2048]{1,0:T(8,128)(2,1)} async-done(((bf16[192,2048]{1,0:T(8,128)(2,1)}), bf16[48,2048]{1,0:T(8,128)(2,1)}) %reduce-scatter.3.cloned.1.call-update) | async-done | bytes 196624 | tf_op jit(solution)/shard_map/reduce_scatter | solution.py:111
  151.1 1.1 multiply_reduce_fusion
  152.2 1.0 multiply_convert_fusion
  153.2 8.0 %all_gather.21 = bf16[192,2048]{1,0:T(8,128)(2,1)S(1)} all-gather(bf16[48,2048]{1,0:T(8,128)(2,1)S(1)} %multiply_convert_fusion), channel_id=1, replica_groups=mesh['sp'=8,'tp'=4] {'tp'}, dimensions={0}, use_global_device_ids=true | all-gather | bytes 983040 | tf_op jit(solution)/shard_map/all_gather | solution.py:120
  161.3 61.3 %all-gather.3.cloned.1.call-done = bf16[2048,1408]{1,0:T(8,128)(2,1)} async-done(((bf16[256,1408]{1,0:T(8,128)(2,1)}), bf16[2048,1408]{1,0:T(8,128)(2,1)}) %all-gather.3.cloned.1.call-update) | async-done | bytes 5767184 | tf_op jit(solution)/shard_map/all_gather | solution.py:123
  222.5 4.0 %fusion.2 = bf16[1,192,1408]{2,1,0:T(8,128)(2,1)S(1)} fusion(bf16[192,2048]{1,0:T(8,128)(2,1)S(1)} %all_gather.21, bf16[2048,1408]{1,0:T(8,128)(2,1)} %all-gather.3.cloned.1.call-done), kind=kOutput, calls=%fused_computation.8 | convolution fusion | flops 1107566592 | bytes 7094272 | tf_op jit(solution)/shard_map/dot_general | solution.py:121
  226.5 88.3 %all-gather.5.cloned.1.call-done = bf16[2048,1408]{1,0:T(8,128)(2,1)} async-done(((bf16[256,1408]{1,0:T(8,128)(2,1)}), bf16[2048,1408]{1,0:T(8,128)(2,1)}) %all-gather.5.cloned.1.call-update) | async-done | bytes 5767184 | tf_op jit(solution)/shard_map/all_gather | solution.py:128
  314.9 4.0 %fusion.3 = bf16[1,192,1408]{2,1,0:T(8,128)(2,1)S(1)} fusion(bf16[192,2048]{1,0:T(8,128)(2,1)S(1)} %all_gather.21, bf16[2048,1408]{1,0:T(8,128)(2,1)} %all-gather.5.cloned.1.call-done), kind=kOutput, calls=%fused_computation.9 | convolution fusion | flops 1107566592 | bytes 7094272 | tf_op jit(solution)/shard_map/dot_general | solution.py:126
  318.9 2.5 collective-permute-start
  321.4 1.3 collective-permute-done
  322.8 0.2 maximum_convert_fusion
  323.0 0.0 slice-start.1
  323.1 0.6 fusion.4
  323.7 1.3 slice-done
  325.0 0.6 slice-done.1
  325.5 2.4 convolution_convert_fusion
  327.9 0.0 reduce-scatter.5.cloned.1.call-update
  327.9 24.1 %reduce-scatter.5.cloned.1.call-done = bf16[48,2048]{1,0:T(8,128)(2,1)} async-done(((bf16[192,2048]{1,0:T(8,128)(2,1)}), bf16[48,2048]{1,0:T(8,128)(2,1)}) %reduce-scatter.5.cloned.1.call-update) | async-done | bytes 196624 | tf_op jit(solution)/shard_map/reduce_scatter | solution.py:140
  352.1 1.7 add_convert_fusion
  (31 shorter events, 0.2 us)
Async XLA Ops:
  7.4 117.7 %copy-start = (bf16[256,2048]{1,0:T(8,128)(2,1)S(1)}, bf16[256,2048]{1,0:T(8,128)(2,1)}, u32[]{:S(2)}) copy-start(bf16[256,2048]{1,0:T(8,128)(2,1)} %param.22) | copy-start | bytes 3145732
  7.4 143.7 %reduce-scatter.3.cloned.1.call-start = ((), (), s32[]{:S(2)}) async-start(), calls=%async_computation.2 | async-start | bytes 983040 | tf_op jit(solution)/shard_map/reduce_scatter | solution.py:111
  7.4 37.6 %copy-start.7 = (bf16[192,128]{1,0:T(8,128)(2,1)S(1)}, bf16[192,128]{1,0:T(8,128)(2,1)}, u32[]{:S(2)}) copy-start(bf16[192,128]{1,0:T(8,128)(2,1)} %param.18) | copy-start | bytes 147460
  80.8 3.2 copy-start.6
  120.3 3.1 copy-start.1
  120.3 3.1 copy-start.2
  120.3 3.1 copy-start.4
  120.3 3.1 copy-start.12
  124.1 0.9 copy-start.11
  125.0 2.6 copy-start.8
  125.0 2.6 copy-start.9
  125.0 26.1 %copy-start.5 = (bf16[192,2048]{1,0:T(8,128)(2,1)S(1)}, bf16[192,2048]{1,0:T(8,128)(2,1)}, u32[]{:S(2)}) copy-start(bf16[192,2048]{1,0:T(8,128)(2,1)} %param.23) | copy-start | bytes 2359300
  125.0 27.1 %copy-start.10 = (f32[2048]{0:T(1024)S(1)}, f32[2048]{0:T(1024)}, u32[]{:S(2)}) copy-start(f32[2048]{0:T(1024)} %param.24) | copy-start | bytes 24580
  126.4 96.1 %all-gather.3.cloned.1.call-start = ((), (), s32[]{:S(2)}) async-start(), calls=%async_computation.3 | async-start | bytes 6488064 | tf_op jit(solution)/shard_map/all_gather | solution.py:123
  127.0 187.9 %all-gather.5.cloned.1.call-start = ((), (), s32[]{:S(2)}) async-start(), calls=%async_computation.4 | async-start | bytes 6488064 | tf_op jit(solution)/shard_map/all_gather | solution.py:128
  127.6 224.5 %reduce-scatter.5.cloned.1.call-start = ((), (), s32[]{:S(2)}) async-start(), calls=%async_computation.5 | async-start | bytes 983040 | tf_op jit(solution)/shard_map/reduce_scatter | solution.py:140
  318.9 3.8 %collective-permute-start = (bf16[2,2,1408]{2,1,0:T(2,128)(2,1)S(1)}, bf16[2,2,1408]{2,1,0:T(2,128)(2,1)S(1)}, u32[]{:S(2)}, u32[]{:S(2)}) collective-permute-start(bf16[2,2,1408]{2,1,0:T(2,128)(2,1)S(1)} %pad_maximum_fusion.2), channel_id=1, source_target_pairs={{0,4},{4,8},{8,12},{12,16},{16,20},{20,24},{24,28},{1,5},{5,9},{9,... | collective-permute-start | bytes 33800 | tf_op jit(solution)/shard_map/ppermute | solution.py:13
  322.8 2.2 slice-start
  323.0 2.5 slice-start.1
  325.5 26.5 %copy-start.3 = (bf16[48,2048]{1,0:T(8,128)(2,1)S(1)}, bf16[48,2048]{1,0:T(8,128)(2,1)}, u32[]{:S(2)}) copy-start(bf16[48,2048]{1,0:T(8,128)(2,1)} %reduce-scatter.3.cloned.1.call-done) | copy-start | bytes 589828
Sparse Core Ops, SparseCore 0:
  126.5 24.5 reduce-scatter.2
  328.0 23.9 reduce-scatter.4
Sparse Core Ops, SparseCore 1:
  129.1 93.4 all-gather.2
  224.6 90.3 all-gather.4
where the time goes:
time: 362 us; the launch traced here: 361 us
  waiting for transfers between devices  200 us (55%)
  blocking collectives  108 us (30%)
  matrix products  18.3 us (5%)
  between operations  15.1 us (4%)
  local copies, waits for them, and re-layouts  8.85 us (2%)
  other arithmetic  8.77 us (2%)
    all_gather x1, waiting for transfers between devices, shards(): lax.all_gather(up_weight, 'sp', axis=0, tiled=True)  88.3 us
    all_gather x1, waiting for transfers between devices, shards(): lax.all_gather(gate_weight, 'sp', axis=0, tiled=True)  61.3 us
    all_gather x1, blocking collectives, shards(): vals = lax.all_gather(values, 'sp', axis=0, tiled=True)  34 us
    all_gather x1, blocking collectives, shards(): keys_b = lax.all_gather(k_second, 'sp', axis=0, tiled=True)  33 us
    all_gather x1, blocking collectives, shards(): keys_a = lax.all_gather(k_first, 'sp', axis=0, tiled=True)  33 us
    reduce_scatter x1, waiting for transfers between devices, shards(): lax.psum_scatter(jnp.dot(hidden, down_weight, preferred_element_type=jnp....  24.1 us
    reduce_scatter x1, waiting for transfers between devices, shards(): lax.psum_scatter(jnp.dot(head_out, out_weight, preferred_element_type=jnp...  23.4 us
    all_gather x1, blocking collectives, shards(): ffn_in = lax.all_gather(normed_part, 'tp', axis=0, tiled=True)  8.02 us
  transfers between devices with their start and end apart: 5, of which 5 were waited for; matrix products, arithmetic and copies ran while one was open for 2% of the time, Pallas kernels for 0%

commit v1 on v0

--- a/solution.py
+++ b/solution.py
@@ -64,8 +64,11 @@
     totals_start = jnp.zeros((head_count, tok_rows), jnp.float32)
     accum_start = jnp.zeros((tok_rows, head_count, value_dim), jnp.float32)
     start = jnp.int32(0)
-    keys_a = lax.all_gather(k_first, "sp", axis=0, tiled=True)
-    keys_b = lax.all_gather(k_second, "sp", axis=0, tiled=True)
+    keys_a, keys_b = jnp.split(
+        lax.all_gather(jnp.concatenate([k_first, k_second], axis=1), "sp", axis=0, tiled=True),
+        [k_first.shape[1]],
+        axis=1,
+    )
     vals = lax.all_gather(values, "sp", axis=0, tiled=True)
     count = keys_a.shape[0]
     span = block_span(count, 2048)

time: 362 us -> 330 us (0.912)
  blocking collectives: 108 us -> 75.9 us
    all_gather x2 -> x1, blocking collectives: 66 us -> 33.9 us  [shards(): lax.all_gather(jnp.concatenate([k_first, k_second], axis=1), 'sp', axis=0...]
    split x0 -> x3, local copies, waits for them, and re-layouts: none -> 3.66 us  [shards(): jnp.split(lax.all_gather(jnp.concatenate([k_first, k_second], axis=1), 's...]
where the time goes in v1:
time: 330 us; the launch traced here: 329 us
  waiting for transfers between devices  200 us (61%)
  blocking collectives  75.9 us (23%)
  matrix products  18.3 us (6%)
  between operations  15.1 us (5%)
  other arithmetic  9.61 us (3%)
  local copies, waits for them, and re-layouts  8.08 us (2%)
    all_gather x1, waiting for transfers between devices, shards(): lax.all_gather(up_weight, 'sp', axis=0, tiled=True)  88.3 us
    all_gather x1, waiting for transfers between devices, shards(): lax.all_gather(gate_weight, 'sp', axis=0, tiled=True)  61.3 us
    all_gather x1, blocking collectives, shards(): vals = lax.all_gather(values, 'sp', axis=0, tiled=True)  34 us
    all_gather x1, blocking collectives, shards(): lax.all_gather(jnp.concatenate([k_first, k_second], axis=1), 'sp', axis=0...  33.9 us
    reduce_scatter x1, waiting for transfers between devices, shards(): lax.psum_scatter(jnp.dot(hidden, down_weight, preferred_element_type=jnp....  24.1 us
    reduce_scatter x1, waiting for transfers between devices, shards(): lax.psum_scatter(jnp.dot(head_out, out_weight, preferred_element_type=jnp...  23.4 us
    all_gather x1, blocking collectives, shards(): ffn_in = lax.all_gather(normed_part, 'tp', axis=0, tiled=True)  8.04 us
  transfers between devices with their start and end apart: 5, of which 5 were waited for; matrix products, arithmetic and copies ran while one was open for 2% of the time, Pallas kernels for 0%

profile of v1, /device:TPU:0, one launch (start us, length us, event | category | flops | bytes accessed | tf_op | source)
XLA Modules:
  0.0 329.1 jit_solution(6240249106945959957)
XLA Ops:
  7.4 0.0 reduce-scatter.3.cloned.1.call-start
  7.4 0.9 iota_compare_fusion
  8.3 0.8 pad_maximum_fusion
  9.2 33.9 %all_gather.15 = bf16[1536,256]{1,0:T(8,128)(2,1)S(1)} all-gather(bf16[192,256]{1,0:T(8,128)(2,1)S(1)} %pad_maximum_fusion), channel_id=1, replica_groups=mesh['sp'=8,'tp'=4] {'sp'}, dimensions={0}, use_global_device_ids=true | all-gather | bytes 884736 | tf_op jit(solution)/shard_map/all_gather | solution.py:68
  43.0 0.8 fusion.56
  43.8 0.9 copy.28
  44.8 0.1 copy.29
  44.9 1.8 fusion.58
  46.7 1.9 copy.32
  48.6 0.0 copy-done.8
  48.6 0.1 copy.33
  48.8 0.0 copy-start.6
  48.8 3.2 fusion.57
  52.0 34.0 %all_gather.16 = bf16[1536,256]{1,0:T(8,128)(2,1)} all-gather(bf16[192,256]{1,0:T(8,128)(2,1)S(1)} %copy-done.6), channel_id=1, replica_groups=mesh['sp'=8,'tp'=4] {'sp'}, dimensions={0}, use_global_device_ids=true | all-gather | bytes 884736 | tf_op jit(solution)/shard_map/all_gather | solution.py:72
  86.0 2.3 copy.30
  88.3 3.0 fusion.8
  91.4 0.7 fusion.43
  92.1 0.0 copy-start.12
  92.1 0.8 multiply_reduce_fusion.1
  92.9 0.0 copy-start.10
  93.0 0.0 copy-start.5
  93.0 0.0 copy-start.11
  93.0 1.3 convolution_convert_fusion.3
  94.3 0.0 reduce-scatter.3.cloned.1.call-update
  94.3 0.0 all-gather.3.cloned.1.call-start
  94.4 0.5 all-gather.3.cloned.1.call-update
  94.9 0.0 all-gather.5.cloned.1.call-start
  95.0 0.5 all-gather.5.cloned.1.call-update
  95.5 0.0 reduce-scatter.5.cloned.1.call-start
  95.6 23.4 %reduce-scatter.3.cloned.1.call-done = bf16[48,2048]{1,0:T(8,128)(2,1)} async-done(((bf16[192,2048]{1,0:T(8,128)(2,1)}), bf16[48,2048]{1,0:T(8,128)(2,1)}) %reduce-scatter.3.cloned.1.call-update) | async-done | bytes 196624 | tf_op jit(solution)/shard_map/reduce_scatter | solution.py:114
  119.0 1.1 multiply_reduce_fusion
  120.1 1.0 multiply_convert_fusion
  121.2 8.0 %all_gather.17 = bf16[192,2048]{1,0:T(8,128)(2,1)S(1)} all-gather(bf16[48,2048]{1,0:T(8,128)(2,1)S(1)} %multiply_convert_fusion), channel_id=1, replica_groups=mesh['sp'=8,'tp'=4] {'tp'}, dimensions={0}, use_global_device_ids=true | all-gather | bytes 983040 | tf_op jit(solution)/shard_map/all_gather | solution.py:123
  129.2 61.3 %all-gather.3.cloned.1.call-done = bf16[2048,1408]{1,0:T(8,128)(2,1)} async-done(((bf16[256,1408]{1,0:T(8,128)(2,1)}), bf16[2048,1408]{1,0:T(8,128)(2,1)}) %all-gather.3.cloned.1.call-update) | async-done | bytes 5767184 | tf_op jit(solution)/shard_map/all_gather | solution.py:126
  190.5 4.0 %fusion.4 = bf16[1,192,1408]{2,1,0:T(8,128)(2,1)S(1)} fusion(bf16[192,2048]{1,0:T(8,128)(2,1)S(1)} %all_gather.17, bf16[2048,1408]{1,0:T(8,128)(2,1)} %all-gather.3.cloned.1.call-done), kind=kOutput, calls=%fused_computation.10 | convolution fusion | flops 1107566592 | bytes 7094272 | tf_op jit(solution)/shard_map/dot_general | solution.py:124
  194.5 88.3 %all-gather.5.cloned.1.call-done = bf16[2048,1408]{1,0:T(8,128)(2,1)} async-done(((bf16[256,1408]{1,0:T(8,128)(2,1)}), bf16[2048,1408]{1,0:T(8,128)(2,1)}) %all-gather.5.cloned.1.call-update) | async-done | bytes 5767184 | tf_op jit(solution)/shard_map/all_gather | solution.py:131
  282.9 4.0 %fusion.5 = bf16[1,192,1408]{2,1,0:T(8,128)(2,1)S(1)} fusion(bf16[192,2048]{1,0:T(8,128)(2,1)S(1)} %all_gather.17, bf16[2048,1408]{1,0:T(8,128)(2,1)} %all-gather.5.cloned.1.call-done), kind=kOutput, calls=%fused_computation.11 | convolution fusion | flops 1107566592 | bytes 7094272 | tf_op jit(solution)/shard_map/dot_general | solution.py:129
  286.9 2.5 collective-permute-start
  289.4 1.3 collective-permute-done
  290.8 0.2 maximum_convert_fusion
  291.0 0.0 slice-start.1
  291.0 0.6 fusion.6
  291.7 1.3 slice-done
  292.9 0.6 slice-done.1
  293.5 2.4 convolution_convert_fusion
  295.9 0.0 reduce-scatter.5.cloned.1.call-update
  295.9 24.1 %reduce-scatter.5.cloned.1.call-done = bf16[48,2048]{1,0:T(8,128)(2,1)} async-done(((bf16[192,2048]{1,0:T(8,128)(2,1)}), bf16[48,2048]{1,0:T(8,128)(2,1)}) %reduce-scatter.5.cloned.1.call-update) | async-done | bytes 196624 | tf_op jit(solution)/shard_map/reduce_scatter | solution.py:143
  320.0 1.7 add_convert_fusion
  (34 shorter events, 0.2 us)
Async XLA Ops:
  7.4 85.6 %copy-start = (bf16[256,2048]{1,0:T(8,128)(2,1)S(1)}, bf16[256,2048]{1,0:T(8,128)(2,1)}, u32[]{:S(2)}) copy-start(bf16[256,2048]{1,0:T(8,128)(2,1)} %param.22) | copy-start | bytes 3145732
  7.4 37.4 %copy-start.7 = (bf16[192,128]{1,0:T(8,128)(2,1)S(1)}, bf16[192,128]{1,0:T(8,128)(2,1)}, u32[]{:S(2)}) copy-start(bf16[192,128]{1,0:T(8,128)(2,1)} %param.15) | copy-start | bytes 147460
  7.4 111.6 %reduce-scatter.3.cloned.1.call-start = ((), (), s32[]{:S(2)}) async-start(), calls=%async_computation.2 | async-start | bytes 983040 | tf_op jit(solution)/shard_map/reduce_scatter | solution.py:114
  43.8 4.8 %copy-start.8 = (bf16[192,128]{1,0:T(8,128)(2,1)S(1)}, bf16[192,128]{1,0:T(8,128)(2,1)}, u32[]{:S(2)}) copy-start(bf16[192,128]{1,0:T(8,128)(2,1)} %param.17) | copy-start | bytes 147460
  48.8 3.2 copy-start.6
  88.3 3.1 copy-start.1
  88.3 3.1 copy-start.2
  88.3 3.1 copy-start.4
  88.3 3.1 copy-start.13
  92.1 0.9 copy-start.12
  92.9 2.6 copy-start.9
  92.9 2.6 copy-start.10
  93.0 26.1 %copy-start.5 = (bf16[192,2048]{1,0:T(8,128)(2,1)S(1)}, bf16[192,2048]{1,0:T(8,128)(2,1)}, u32[]{:S(2)}) copy-start(bf16[192,2048]{1,0:T(8,128)(2,1)} %param.23) | copy-start | bytes 2359300
  93.0 27.1 %copy-start.11 = (f32[2048]{0:T(1024)S(1)}, f32[2048]{0:T(1024)}, u32[]{:S(2)}) copy-start(f32[2048]{0:T(1024)} %param.24) | copy-start | bytes 24580
  94.3 96.1 %all-gather.3.cloned.1.call-start = ((), (), s32[]{:S(2)}) async-start(), calls=%async_computation.3 | async-start | bytes 6488064 | tf_op jit(solution)/shard_map/all_gather | solution.py:126
  94.9 187.9 %all-gather.5.cloned.1.call-start = ((), (), s32[]{:S(2)}) async-start(), calls=%async_computation.4 | async-start | bytes 6488064 | tf_op jit(solution)/shard_map/all_gather | solution.py:131
  95.5 224.5 %reduce-scatter.5.cloned.1.call-start = ((), (), s32[]{:S(2)}) async-start(), calls=%async_computation.5 | async-start | bytes 983040 | tf_op jit(solution)/shard_map/reduce_scatter | solution.py:143
  286.9 3.8 %collective-permute-start = (bf16[2,2,1408]{2,1,0:T(2,128)(2,1)S(1)}, bf16[2,2,1408]{2,1,0:T(2,128)(2,1)S(1)}, u32[]{:S(2)}, u32[]{:S(2)}) collective-permute-start(bf16[2,2,1408]{2,1,0:T(2,128)(2,1)S(1)} %pad_maximum_fusion.3), channel_id=1, source_target_pairs={{0,4},{4,8},{8,12},{12,16},{16,20},{20,24},{24,28},{1,5},{5,9},{9,... | collective-permute-start | bytes 33800 | tf_op jit(solution)/shard_map/ppermute | solution.py:13
  290.8 2.2 slice-start
  291.0 2.5 slice-start.1
  293.5 26.5 %copy-start.3 = (bf16[48,2048]{1,0:T(8,128)(2,1)S(1)}, bf16[48,2048]{1,0:T(8,128)(2,1)}, u32[]{:S(2)}) copy-start(bf16[48,2048]{1,0:T(8,128)(2,1)} %reduce-scatter.3.cloned.1.call-done) | copy-start | bytes 589828
Sparse Core Ops, SparseCore 0:
  94.5 24.5 reduce-scatter.2
  296.0 23.9 reduce-scatter.4
Sparse Core Ops, SparseCore 1:
  97.0 93.4 all-gather.2
  192.5 90.3 all-gather.4
